TPU v7x, 768 devices: a whole 4x8x12 slice. The times are simulated.
768 devices in a mesh: ra: 24 (over z, core), cb: 32 (over y, x).
Axes of the slice: x: 4, y: 8, z: 12, core: 2. Of those that a mesh axis runs over, the one named last changes fastest.
Arguments:
- tokens: bfloat16 [2, 128, 3072], P(None, None, 'ra'), may hold values from -70 to 70
- norm_gain: float32 [2, 3072], P(None, 'ra'), may hold values from 0.1 to 1.9
- gate_weight: float32 [2, 3072, 8448], P(None, 'ra', 'cb'), may hold values from -0.109375 to 0.109375
- gate_scale: float32 [2, 8448], P(None, 'cb'), may hold values from 0.5 to 2
- up_weight: float32 [2, 3072, 8448], P(None, 'ra', 'cb'), may hold values from -0.109375 to 0.109375
- up_scale: float32 [2, 8448], P(None, 'cb'), may hold values from 0.5 to 2
- conv_weight: float32 [2, 3, 8448], P(None, None, 'cb'), may hold values from -3.5 to 3.5
- conv_bias: float32 [2, 8448], P(None, 'cb'), may hold values from -3 to 3
- down_weight: float32 [2, 8448, 3072], P(None, 'cb', 'ra'), may hold values from -0.0625 to 0.0625
- down_scale: float32 [2, 3072], P(None, 'ra'), may hold values from 0.5 to 2
Outputs:
- layer_output: bfloat16 [2, 128, 3072], P(None, None, 'ra')
All inputs are finite; a program needn't handle non-finite values.
Results may differ from a plain program's by a relative error of at most 0.014.
Values may be sent and summed in bfloat16 or wider, within the bound.
A program may use at most 32 MiB of HBM per device.

v0:
```python
import jax
import jax.numpy as jnp
from jax import lax
from jax.sharding import Mesh
from jax.sharding import PartitionSpec as P

WIDTH = 3072
CB = ("cb_0", "cb_1")


eps = 1e-06
residual_keep = 0.5


def cut_along(x, dim, length):
    before, after = (x.shape[:dim], x.shape[dim + 1 :])
    return jnp.moveaxis(x.reshape(*before, length, -1, *after), dim, 0)


def sent_and_summed(x, axis, dim):
    tiles = cut_along(x, dim, lax.axis_size(axis))
    arrived = lax.all_to_all(tiles, axis, split_axis=0, concat_axis=0, tiled=True)
    return arrived.sum(axis=0)


def in_one_piece(arrays, axis, dim, along):
    ends, at = ([], 0)
    for a in arrays[:-1]:
        at += a.shape[along]
        ends.append(at)
    both = jnp.concatenate(arrays, axis=along)
    return tuple(jnp.split(sent_and_summed(both, axis, dim), ends, axis=along))


def sent_to_all(x, axis):
    length = lax.axis_size(axis)
    return lax.all_to_all(jnp.broadcast_to(x[None], (length, *x.shape)), axis, 0, 0, tiled=True)


def taken_together(x, axis):
    return sent_to_all(x, axis).sum(axis=0)


def joined_along(tiles, dim):
    shape = list(tiles.shape[1:])
    shape[dim] *= tiles.shape[0]
    return jnp.moveaxis(tiles, 0, dim).reshape(shape)


def collect(x, axis, dim):
    tiles = sent_to_all(x, axis)
    return joined_along(tiles, dim)


def filled_up(lines, length):
    spare = -lines.shape[0] % length
    if not spare:
        return lines
    return jnp.concatenate([lines, jnp.zeros((spare, *lines.shape[1:]), lines.dtype)])


def reduced_to_own(tiles, axes, order):
    shape = [lax.axis_size(a) for a in axes]
    tiles = tiles.reshape(*shape, *tiles.shape[1:])
    tiles = tiles.transpose(*order, *range(len(axes), tiles.ndim))
    tiles = tiles.reshape(-1, *tiles.shape[len(axes) :])
    for k in order:
        tiles = lax.psum_scatter(tiles, axes[k], scatter_dimension=0, tiled=True)
    return tiles[0]


def gather_in_order(x, axes, order):
    tiles = x[None]
    for k in order:
        tiles = lax.all_gather(tiles, axes[k], axis=0, tiled=True)
    current = [lax.axis_size(axes[k]) for k in reversed(order)]
    tiles = tiles.reshape(*current, *x.shape)
    turned = sorted(range(len(order)), key=lambda place: order[len(order) - 1 - place])
    return tiles.transpose(*turned, *range(len(order), tiles.ndim)).reshape(-1, *x.shape)


def total_of(x, axes, order):
    length, lines = (lax.axis_size(axes), x.reshape(-1, *x.shape[1:][-1:]))
    tiles = filled_up(lines, length).reshape(length, -1, *lines.shape[1:])
    own = reduced_to_own(tiles, axes, order)
    whole = gather_in_order(own, axes, order[::-1]).reshape(-1, *lines.shape[1:])
    return whole[: len(lines)].reshape(x.shape)


def causal_mix(gate_seq, conv_taps, conv_shift):
    count = conv_taps.shape[0]
    length = gate_seq.shape[1]
    padded = jnp.pad(gate_seq, ((0, 0), (count - 1, 0), (0, 0)))
    running = jnp.zeros_like(gate_seq) + conv_shift[None, None, :]
    for offset in range(count):
        running = (
            running + conv_taps[offset][None, None, :] * padded[:, offset : offset + length, :]
        )
    return running


def sublayer(current, norm_g, gate_w, gate_s, up_w, up_s, conv_taps, conv_shift, down_w, down_s):
    sequences, length, local_width = current.shape
    row_count = sequences * length
    values = current.astype(jnp.float32).reshape(row_count, local_width)
    squares = jnp.sum(values * values, axis=1)
    scaled = (values * norm_g[None, :]).astype(jnp.bfloat16)
    gate_part = jnp.dot(scaled, gate_w.astype(jnp.bfloat16), preferred_element_type=jnp.float32)
    up_part = jnp.dot(scaled, up_w.astype(jnp.bfloat16), preferred_element_type=jnp.float32)
    gate_sum, up_sum = in_one_piece((gate_part, up_part), "ra", 1, 0)
    square_sum = taken_together(squares, "ra")
    share_cols = gate_sum.shape[1]
    col_start = lax.axis_index("ra") * share_cols
    col_gate = lax.dynamic_slice_in_dim(gate_s, col_start, share_cols, 0)
    col_up = lax.dynamic_slice_in_dim(up_s, col_start, share_cols, 0)
    used_taps = lax.dynamic_slice_in_dim(conv_taps, col_start, share_cols, 1)
    used_shift = lax.dynamic_slice_in_dim(conv_shift, col_start, share_cols, 0)
    inverse_rms = lax.rsqrt(square_sum / WIDTH + eps)[:, None]
    gate_sum = gate_sum * inverse_rms * col_gate[None, :]
    up_sum = up_sum * inverse_rms * col_up[None, :]
    units = gate_sum.shape[1]
    conv_out = causal_mix(gate_sum.reshape(sequences, length, units), used_taps, used_shift)
    hidden_act = (jax.nn.silu(conv_out) * up_sum.reshape(sequences, length, units)).astype(
        jnp.bfloat16
    )
    hidden_act = hidden_act.reshape(row_count, units)
    hidden_act = collect(hidden_act, "ra", 1)
    down_part = jnp.dot(hidden_act, down_w.astype(jnp.bfloat16), preferred_element_type=jnp.float32)
    down_sum = total_of(down_part, CB, (0, 1))
    branch = down_sum * down_s[None, :]
    return (
        (residual_keep * values + branch)
        .astype(jnp.bfloat16)
        .reshape(sequences, length, local_width)
    )


def shards(
    tokens,
    norm_gain,
    gate_weight,
    gate_scale,
    up_weight,
    up_scale,
    conv_weight,
    conv_bias,
    down_weight,
    down_scale,
):
    current = tokens
    for layer_index in range(2):
        current = sublayer(
            current,
            norm_gain[layer_index],
            gate_weight[layer_index],
            gate_scale[layer_index],
            up_weight[layer_index],
            up_scale[layer_index],
            conv_weight[layer_index],
            conv_bias[layer_index],
            down_weight[layer_index],
            down_scale[layer_index],
        )
    return current


def solution(mesh):
    split = Mesh(mesh.devices.reshape(mesh.shape["ra"], 8, 4), ("ra", "cb_0", "cb_1"))
    in_specs = (
        P(None, None, "ra"),
        P(None, "ra"),
        P(None, "ra", CB),
        P(None, CB),
        P(None, "ra", CB),
        P(None, CB),
        P(None, None, CB),
        P(None, CB),
        P(None, CB, "ra"),
        P(None, "ra"),
    )
    out_specs = P(None, None, "ra")
    return jax.shard_map(
        shards, mesh=split, in_specs=in_specs, out_specs=out_specs, check_vma=False
    )
```

profile of v0, /device:TPU:24, one launch (start us, length us, event | category | flops | bytes accessed | tf_op | source)
XLA Modules:
  0.0 359.0 jit_solution(17556408786695192732)
XLA Ops:
  6.5 0.8 slice_bitcast_fusion.13
  7.3 0.9 fusion.3
  8.9 15.4 %all-to-all-start.1 = ((f32[24,1,256]{2,1,0:T(1,128)}), f32[24,1,256]{2,1,0:T(1,128)S(1)}, u32[]{:S(2)}, u32[]{:S(2)}) async-start(f32[24,1,256]{2,1,0:T(1,128)} %broadcast_in_dim.17), calls=%async_computation.1 | async-start | bytes 49152 | tf_op jit(solution)/shard_map/all_to_all | solution.py:37
  24.3 1.0 convert.13
  25.2 1.0 convert.12
  26.8 1.0 reshape.130
  27.7 6.5 %all-to-all-done.1 = f32[24,1,256]{2,1,0:T(1,128)S(1)} async-done(((f32[24,1,256]{2,1,0:T(1,128)}), f32[24,1,256]{2,1,0:T(1,128)S(1)}, u32[]{:S(2)}, u32[]{:S(2)}) %all-to-all-start.1) | async-done | bytes 24608 | tf_op jit(solution)/shard_map/all_to_all | solution.py:37
  34.2 4.0 %all-to-all-start = ((f32[24,512,11]{1,2,0:T(8,128)}), f32[24,512,11]{1,2,0:T(8,128)S(1)}, u32[]{:S(2)}, u32[]{:S(2)}) async-start(f32[24,512,11]{1,2,0:T(8,128)} %bitcast.6), calls=%async_computation | async-start | bytes 1572864 | tf_op jit(solution)/shard_map/all_to_all | solution.py:22
  38.7 32.7 %all-to-all-done = f32[24,512,11]{1,2,0:T(8,128)S(1)} async-done(((f32[24,512,11]{1,2,0:T(8,128)}), f32[24,512,11]{1,2,0:T(8,128)S(1)}, u32[]{:S(2)}, u32[]{:S(2)}) %all-to-all-start) | async-done | bytes 540704 | tf_op jit(solution)/shard_map/all_to_all | solution.py:22
  72.4 3.8 %all-to-all-start.2 = ((bf16[24,256,11]{1,2,0:T(8,128)(2,1)}), bf16[24,256,11]{1,2,0:T(8,128)(2,1)S(1)}, u32[]{:S(2)}, u32[]{:S(2)}) async-start(bf16[24,256,11]{1,2,0:T(8,128)(2,1)} %broadcast_in_dim.19), calls=%async_computation.2 | async-start | bytes 393216 | tf_op jit(solution)/shard_map/all_to_all | solution.py:37
  76.3 14.6 %all-to-all-done.2 = bf16[24,256,11]{1,2,0:T(8,128)(2,1)S(1)} async-done(((bf16[24,256,11]{1,2,0:T(8,128)(2,1)}), bf16[24,256,11]{1,2,0:T(8,128)(2,1)S(1)}, u32[]{:S(2)}, u32[]{:S(2)}) %all-to-all-start.2) | async-done | bytes 135200 | tf_op jit(solution)/shard_map/all_to_all | solution.py:37
  90.8 1.0 copy.16
  91.8 0.9 dot_general.24
  92.7 0.9 fusion.11
  93.6 1.3 dynamic-slice.8
  94.9 35.1 %reduce-scatter.3.cloned.1.call-done = f32[4,8,128]{2,1,0:T(8,128)} async-done(((f32[32,8,128]{2,1,0:T(8,128)}), f32[4,8,128]{2,1,0:T(8,128)}) %reduce-scatter.3.cloned.1.call-update) | async-done | bytes 16400 | tf_op jit(solution)/shard_map/reduce_scatter | solution.py:68
  130.0 17.4 %all-reduce.2 = f32[4,8,128]{2,1,0:T(8,128)S(1)} all-reduce(f32[4,8,128]{2,1,0:T(8,128)} %reduce-scatter.3.cloned.1.call-done), channel_id=3, replica_groups=mesh['ra'=24,'cb_0'=8,'cb_1'=4] {'cb_1'}, use_global_device_ids=true, to_apply=%region_4.5.clone | all-reduce | flops 4096 | bytes 32768
  148.1 12.0 %all_gather.12 = f32[4,8,128]{2,1,0:T(8,128)S(1)} all-gather(f32[1,8,128]{2,1,0:T(8,128)S(1)} %constant_dynamic-slice_fusion.13), channel_id=1, replica_groups=mesh['ra'=24,'cb_0'=8,'cb_1'=4] {'cb_1'}, dimensions={0}, use_global_device_ids=true | all-gather | bytes 20480 | tf_op jit(solution)/shard_map/all_gather | solution.py:75
  160.1 24.6 %all_gather.13 = f32[32,8,128]{2,1,0:T(8,128)S(1)} all-gather(f32[4,8,128]{2,1,0:T(8,128)S(1)} %all_gather.12), channel_id=1, replica_groups=mesh['ra'=24,'cb_0'=8,'cb_1'=4] {'cb_0'}, dimensions={0}, use_global_device_ids=true | all-gather | bytes 147456 | tf_op jit(solution)/shard_map/all_gather | solution.py:75
  185.9 10.4 %all-to-all-start.4 = ((f32[24,1,256]{2,1,0:T(1,128)}), f32[24,1,256]{2,1,0:T(1,128)S(1)}, u32[]{:S(2)}, u32[]{:S(2)}) async-start(f32[24,1,256]{2,1,0:T(1,128)} %broadcast_in_dim.21), calls=%async_computation.5 | async-start | bytes 49152 | tf_op jit(solution)/shard_map/all_to_all | solution.py:37
  196.4 1.0 reshape.133
  197.3 8.9 %all-to-all-done.4 = f32[24,1,256]{2,1,0:T(1,128)S(1)} async-done(((f32[24,1,256]{2,1,0:T(1,128)}), f32[24,1,256]{2,1,0:T(1,128)S(1)}, u32[]{:S(2)}, u32[]{:S(2)}) %all-to-all-start.4) | async-done | bytes 24608 | tf_op jit(solution)/shard_map/all_to_all | solution.py:37
  206.3 3.9 %all-to-all-start.3 = ((f32[24,512,11]{1,2,0:T(8,128)}), f32[24,512,11]{1,2,0:T(8,128)S(1)}, u32[]{:S(2)}, u32[]{:S(2)}) async-start(f32[24,512,11]{1,2,0:T(8,128)} %bitcast.23), calls=%async_computation.4 | async-start | bytes 1572864 | tf_op jit(solution)/shard_map/all_to_all | solution.py:22
  210.4 32.9 %all-to-all-done.3 = f32[24,512,11]{1,2,0:T(8,128)S(1)} async-done(((f32[24,512,11]{1,2,0:T(8,128)}), f32[24,512,11]{1,2,0:T(8,128)S(1)}, u32[]{:S(2)}, u32[]{:S(2)}) %all-to-all-start.3) | async-done | bytes 540704 | tf_op jit(solution)/shard_map/all_to_all | solution.py:22
  243.6 17.9 %all_to_all.32 = bf16[24,256,11]{1,2,0:T(8,128)(2,1)S(1)} all-to-all(bf16[24,256,11]{1,2,0:T(8,128)(2,1)S(1)} %broadcast_in_dim.45), channel_id=1, replica_groups=mesh['ra'=24,'cb_0'=8,'cb_1'=4] {'ra'}, dimensions={0} | all-to-all | bytes 270336 | tf_op jit(solution)/shard_map/all_to_all | solution.py:37
  261.5 1.0 copy.18
  262.5 0.8 dot_general.28
  263.3 0.9 fusion.8
  264.2 32.6 %reduce-scatter.5.cloned.1.call-done = f32[4,8,128]{2,1,0:T(8,128)} async-done(((f32[32,8,128]{2,1,0:T(8,128)}), f32[4,8,128]{2,1,0:T(8,128)}) %reduce-scatter.5.cloned.1.call-update) | async-done | bytes 16400 | tf_op jit(solution)/shard_map/reduce_scatter | solution.py:68
  296.8 17.4 %all-reduce.3 = f32[4,8,128]{2,1,0:T(8,128)S(1)} all-reduce(f32[4,8,128]{2,1,0:T(8,128)} %reduce-scatter.5.cloned.1.call-done), channel_id=5, replica_groups=mesh['ra'=24,'cb_0'=8,'cb_1'=4] {'cb_1'}, use_global_device_ids=true, to_apply=%region_9.10.clone | all-reduce | flops 4096 | bytes 32768
  314.9 12.0 %all_gather.14 = f32[4,8,128]{2,1,0:T(8,128)S(1)} all-gather(f32[1,8,128]{2,1,0:T(8,128)S(1)} %constant_dynamic-slice_fusion.12), channel_id=1, replica_groups=mesh['ra'=24,'cb_0'=8,'cb_1'=4] {'cb_1'}, dimensions={0}, use_global_device_ids=true | all-gather | bytes 20480 | tf_op jit(solution)/shard_map/all_gather | solution.py:75
  326.9 24.6 %all_gather.15 = f32[32,8,128]{2,1,0:T(8,128)S(1)} all-gather(f32[4,8,128]{2,1,0:T(8,128)S(1)} %all_gather.14), channel_id=1, replica_groups=mesh['ra'=24,'cb_0'=8,'cb_1'=4] {'cb_0'}, dimensions={0}, use_global_device_ids=true | all-gather | bytes 147456 | tf_op jit(solution)/shard_map/all_gather | solution.py:75
  (61 shorter events, 6.2 us)
Async XLA Ops:
  8.9 25.4 %all-to-all-start.1 = ((f32[24,1,256]{2,1,0:T(1,128)}), f32[24,1,256]{2,1,0:T(1,128)S(1)}, u32[]{:S(2)}, u32[]{:S(2)}) async-start(f32[24,1,256]{2,1,0:T(1,128)} %broadcast_in_dim.17), calls=%async_computation.1 | async-start | bytes 49152 | tf_op jit(solution)/shard_map/all_to_all | solution.py:37
  26.7 11.6 %copy-start.3 = (f32[2,264]{1,0:T(2,128)S(1)}, f32[2,264]{1,0:T(2,128)}, u32[]{:S(2)}) copy-start(f32[2,264]{1,0:T(2,128)} %param.13) | copy-start | bytes 6340
  26.7 11.6 %copy-start.4 = (f32[2,264]{1,0:T(2,128)S(1)}, f32[2,264]{1,0:T(2,128)}, u32[]{:S(2)}) copy-start(f32[2,264]{1,0:T(2,128)} %param.15) | copy-start | bytes 6340
  26.7 11.7 %copy-start.5 = (f32[2,264]{1,0:T(2,128)S(1)}, f32[2,264]{1,0:T(2,128)}, u32[]{:S(2)}) copy-start(f32[2,264]{1,0:T(2,128)} %param.17) | copy-start | bytes 6340
  26.8 11.7 %copy-start.2 = (f32[2,3,264]{2,0,1:T(2,128)S(1)}, f32[2,3,264]{2,0,1:T(2,128)}, u32[]{:S(2)}) copy-start(f32[2,3,264]{2,0,1:T(2,128)} %param.16) | copy-start | bytes 19012
  34.2 42.0 %copy-start = (f32[2,264,128]{2,1,0:T(8,128)S(1)}, f32[2,264,128]{2,1,0:T(8,128)}, u32[]{:S(2)}) copy-start(f32[2,264,128]{2,1,0:T(8,128)} %param.18) | copy-start | bytes 811012
  34.2 37.1 %all-to-all-start = ((f32[24,512,11]{1,2,0:T(8,128)}), f32[24,512,11]{1,2,0:T(8,128)S(1)}, u32[]{:S(2)}, u32[]{:S(2)}) async-start(f32[24,512,11]{1,2,0:T(8,128)} %bitcast.6), calls=%async_computation | async-start | bytes 1572864 | tf_op jit(solution)/shard_map/all_to_all | solution.py:22
  72.4 18.5 %all-to-all-start.2 = ((bf16[24,256,11]{1,2,0:T(8,128)(2,1)}), bf16[24,256,11]{1,2,0:T(8,128)(2,1)S(1)}, u32[]{:S(2)}, u32[]{:S(2)}) async-start(bf16[24,256,11]{1,2,0:T(8,128)(2,1)} %broadcast_in_dim.19), calls=%async_computation.2 | async-start | bytes 393216 | tf_op jit(solution)/shard_map/all_to_all | solution.py:37
  76.2 53.8 %reduce-scatter.3.cloned.1.call-start = ((), (), s32[]{:S(2)}) async-start(), calls=%async_computation.8 | async-start | bytes 147456 | tf_op jit(solution)/shard_map/reduce_scatter | solution.py:68
  91.8 3.1 copy-start.6
  91.8 92.8 %copy-start.1 = (bf16[2,128,128]{2,1,0:T(8,128)(2,1)S(1)}, bf16[2,128,128]{2,1,0:T(8,128)(2,1)}, u32[]{:S(2)}) copy-start(bf16[2,128,128]{2,1,0:T(8,128)(2,1)} %param.10) | copy-start | bytes 196612
  185.9 20.4 %all-to-all-start.4 = ((f32[24,1,256]{2,1,0:T(1,128)}), f32[24,1,256]{2,1,0:T(1,128)S(1)}, u32[]{:S(2)}, u32[]{:S(2)}) async-start(f32[24,1,256]{2,1,0:T(1,128)} %broadcast_in_dim.21), calls=%async_computation.5 | async-start | bytes 49152 | tf_op jit(solution)/shard_map/all_to_all | solution.py:37
  206.3 36.9 %all-to-all-start.3 = ((f32[24,512,11]{1,2,0:T(8,128)}), f32[24,512,11]{1,2,0:T(8,128)S(1)}, u32[]{:S(2)}, u32[]{:S(2)}) async-start(f32[24,512,11]{1,2,0:T(8,128)} %bitcast.23), calls=%async_computation.4 | async-start | bytes 1572864 | tf_op jit(solution)/shard_map/all_to_all | solution.py:22
  210.2 86.6 %reduce-scatter.5.cloned.1.call-start = ((), (), s32[]{:S(2)}) async-start(), calls=%async_computation.9 | async-start | bytes 147456 | tf_op jit(solution)/shard_map/reduce_scatter | solution.py:68
Sparse Core Ops, SparseCore 0:
  93.7 36.2 reduce-scatter.2
  264.3 32.4 reduce-scatter.4
where the time goes:
time: 360 us; the launch traced here: 359 us
  waiting for transfers between devices  163 us (45%)
  blocking collectives  126 us (35%)
  starting transfers between devices  37.6 us (10%)
  between operations  13.8 us (4%)
  local copies, waits for them, and re-layouts  11.3 us (3%)
  other arithmetic  4.51 us (1%)
    all_gather x4, blocking collectives, gather_in_order(): tiles = lax.all_gather(tiles, axes[k], axis=0, tiled=True)  73.2 us
    reduce_scatter x2, waiting for transfers between devices, reduced_to_own(): tiles = lax.psum_scatter(tiles, axes[k], scatter_dimension=0, tiled=True)  67.7 us
    all_to_all x2, waiting for transfers between devices, sent_and_summed(): lax.all_to_all(tiles, axis, split_axis=0, concat_axis=0, tiled=True)  65.5 us
    unnamed x2, blocking collectives  34.9 us
    all_to_all x3, waiting for transfers between devices, sent_to_all(): lax.all_to_all(jnp.broadcast_to(x[None], (length, *x.shape)), axis, 0, 0,...  30 us
    all_to_all x3, starting transfers between devices, sent_to_all(): lax.all_to_all(jnp.broadcast_to(x[None], (length, *x.shape)), axis, 0, 0,...  29.6 us
    all_to_all x1, blocking collectives, sent_to_all(): lax.all_to_all(jnp.broadcast_to(x[None], (length, *x.shape)), axis, 0, 0,...  17.9 us
    all_to_all x2, starting transfers between devices, sent_and_summed(): lax.all_to_all(tiles, axis, split_axis=0, concat_axis=0, tiled=True)  7.92 us
  transfers between devices with their start and end apart: 7, of which 7 were waited for; matrix products, arithmetic and copies ran while one was open for 2% of the time, Pallas kernels for 0%

commit v1 on v0

v1 whole, which is shorter than its diff:
```python
import functools

import jax
import jax.numpy as jnp
from jax import lax
from jax.experimental import pallas as pl
from jax.experimental.pallas import tpu as pltpu
from jax.sharding import PartitionSpec as P

EPS = 1e-06
KEEP = 0.5
F32 = jnp.float32
BF16 = jnp.bfloat16
MESH = pl.DeviceIdType.MESH


def nt(a, b, precision=None):
    return lax.dot_general(
        a, b, (((1,), (1,)), ((), ())), preferred_element_type=F32, precision=precision
    )


def nn(a, b):
    return lax.dot_general(a, b, (((1,), (0,)), ((), ())), preferred_element_type=F32)


def ring_offsets(n):
    return sorted(range(1, n), key=lambda d: -min(d, n - d))


def plane_offsets(ny, nx):
    away = lambda p: min(p[0], ny - p[0]) + min(p[1], nx - p[1])
    return sorted(
        ((dy, dx) for dy in range(ny) for dx in range(nx) if dy or dx), key=lambda p: -away(p)
    )


def kernel(
    cfg,
    tok_h, g_h, wg_h, gs_h, wu_h, us_h, cw_h, cbias_h, wd_h, ds_h,
    out_ref,
    tok, g, wg, gs, wu, us, cw, cbias, wd, ds,
    xt_send, hT, gT, dsT, w1, w2, prm,
    s1, r1, r2, s3, r3, hn_send, fin,
    load_sem, ex_send, ex_recv, ph_send, ph_recv,
):
    NZ, NY, NX, FC, U, UP, T, width = cfg
    NB = NY * NX
    UZ = U // NZ
    FB = 2 * FC // NB
    HB = NB // 2
    ra = lax.axis_index("ra")
    cb = lax.axis_index("cb")
    z = lax.div(ra, 2)
    c = lax.rem(ra, 2)
    o = 1 - c
    y = lax.div(cb, NX)
    x = lax.rem(cb, NX)

    barrier = pltpu.get_barrier_semaphore()

    def zpeer(d):
        return (2 * lax.rem(z + d, NZ) + c, cb)

    def plane_index(off):
        return lax.rem(y + off[0], NY) * NX + lax.rem(x + off[1], NX)

    ring = ring_offsets(NZ)
    plane = plane_offsets(NY, NX)
    peers = [zpeer(d) for d in ring] + [(ra, plane_index(p)) for p in plane]
    peers += [(2 * z + o, plane_index(p)) for p in plane] + [(2 * z + o, cb)]
    for peer in peers:
        pl.semaphore_signal(barrier, inc=1, device_id=peer, device_id_type=MESH)

    pairs = [
        (tok_h, tok), (g_h, g), (wg_h, wg), (wu_h, wu), (gs_h, gs), (us_h, us),
        (cw_h, cw), (cbias_h, cbias), (wd_h, wd), (ds_h, ds),
    ]
    loads = [
        pltpu.make_async_copy(src, dst, load_sem.at[i]) for i, (src, dst) in enumerate(pairs)
    ]
    for load in loads:
        load.start()

    own_half = pl.ds(pl.multiple_of(c * FC, FC), FC)
    own_slots = pl.ds(c * HB, HB)

    def column_tile(row):
        return jnp.transpose(jnp.broadcast_to(row, (T, FC)))

    loads[0].wait()
    mine = jnp.transpose(tok[c].astype(F32)).reshape(HB, FB, T).astype(BF16)
    hT[0, own_slots] = mine
    xt_send[...] = jnp.transpose(tok[o].astype(F32)).reshape(HB, FB, T).astype(BF16)
    loads[1].wait()
    for l in range(2):
        gT[l, own_half, :] = column_tile(g[l : l + 1, :])

    row = lax.broadcasted_iota(jnp.int32, (NZ * 2 * UP, U), 0)
    col = lax.broadcasted_iota(jnp.int32, (NZ * 2 * UP, U), 1)
    block = lax.div(row, 2 * UP)
    inner = row - block * (2 * UP)
    pick_g = ((inner < UZ) & (col == block * UZ + inner)).astype(F32).astype(BF16)
    upper = inner - UP
    pick_u = (
        ((upper >= 0) & (upper < UZ) & (col == block * UZ + upper)).astype(F32).astype(BF16)
    )

    def arrange_in(l):
        w1[l, c] = (nt(pick_g, wg[l].astype(BF16)) + nt(pick_u, wu[l].astype(BF16))).astype(BF16)

    loads[2].wait()
    loads[3].wait()
    arrange_in(0)

    def to_partner(k, src, dst):
        return pltpu.make_async_remote_copy(
            src_ref=src,
            dst_ref=dst,
            send_sem=ex_send.at[k],
            recv_sem=ex_recv.at[k],
            device_id=(2 * z + o, cb),
            device_id_type=MESH,
        )

    ex = [
        to_partner(0, xt_send, hT.at[0, own_slots]),
        to_partner(1, gT.at[0, own_half, :], gT.at[0, own_half, :]),
        to_partner(2, w1.at[0, c], w1.at[0, c]),
        to_partner(3, w2.at[0, own_half, :], w2.at[0, own_half, :]),
        to_partner(4, dsT.at[:, own_half, :], dsT.at[:, own_half, :]),
        to_partner(5, gT.at[1, own_half, :], gT.at[1, own_half, :]),
        to_partner(6, w1.at[1, c], w1.at[1, c]),
        to_partner(7, w2.at[1, own_half, :], w2.at[1, own_half, :]),
    ]

    pl.semaphore_wait(barrier, len(peers))
    for k in range(3):
        ex[k].start()

    def prepare_rest():
        for k in range(4, 10):
            loads[k].wait()
        rows = [gs[0:1, :], gs[1:2, :], us[0:1, :], us[1:2, :], cbias[0:1, :], cbias[1:2, :]]
        rows += [cw[0, j : j + 1, :] for j in range(3)] + [cw[1, j : j + 1, :] for j in range(3)]
        rows += [jnp.zeros((16 - len(rows), U), F32)]
        table = jnp.concatenate(rows, axis=0)
        unit = lax.broadcasted_iota(jnp.int32, (UP, U), 0)
        at = lax.broadcasted_iota(jnp.int32, (UP, U), 1)
        own = ((unit < UZ) & (at == z * UZ + unit)).astype(F32)
        picked = nt(own, table, precision=lax.Precision.HIGHEST)
        for k in range(12):
            prm[k] = jnp.broadcast_to(picked[:, k : k + 1], (UP, T))
        for l in range(2):
            dsT[l, own_half, :] = column_tile(ds[l : l + 1, :])
        urow = lax.broadcasted_iota(jnp.int32, (NZ * UP, U), 0)
        ucol = lax.broadcasted_iota(jnp.int32, (NZ * UP, U), 1)
        ublock = lax.div(urow, UP)
        uin = urow - ublock * UP
        pick_d = ((uin < UZ) & (ucol == ublock * UZ + uin)).astype(F32).astype(BF16)
        eye = (
            lax.broadcasted_iota(jnp.int32, (FC, FC), 0)
            == lax.broadcasted_iota(jnp.int32, (FC, FC), 1)
        ).astype(F32).astype(BF16)
        for l in range(2):
            arranged = nn(pick_d, wd[l].astype(BF16)).astype(BF16)
            w2[l, own_half, :] = nt(eye, arranged).astype(BF16)
            if l == 0:
                ex[3].start()
                ex[4].start()
        arrange_in(1)
        for k in range(5, 8):
            ex[k].start()

    lane = lax.broadcasted_iota(jnp.int32, (UP, T), 1)

    def shifted(v, by):
        return jnp.where(lane >= by, pltpu.roll(v, by, 1), 0.0)

    def remote(l, p, src, dst, peer):
        return pltpu.make_async_remote_copy(
            src_ref=src,
            dst_ref=dst,
            send_sem=ph_send.at[l, p],
            recv_sem=ph_recv.at[l, p],
            device_id=peer,
            device_id_type=MESH,
        )

    def wait_bytes(sem, ref):
        pltpu.make_async_copy(ref, ref, sem).wait()

    for l in range(2):
        for k in (range(3) if l == 0 else range(5, 7)):
            ex[k].wait_recv()
        h = hT[l].astype(F32).reshape(2 * FC, T)
        squares = jnp.sum(h * h, axis=0, keepdims=True)
        scaled = (h * gT[l]).astype(BF16)
        both = jnp.concatenate([w1[l, 0], w1[l, 1]], axis=1)
        part = nn(both, scaled).reshape(NZ, 2 * UP, T)
        high = squares.astype(BF16).astype(F32)
        low = squares - high
        sub = lax.broadcasted_iota(jnp.int32, (2 * UP, T), 0)
        extra = jnp.where(sub == UZ, high, 0.0) + jnp.where(sub == UZ + 1, low, 0.0)
        part = (part + extra[None]).astype(BF16)
        s1[l] = part
        for d in ring:
            to = lax.rem(z + d, NZ)
            remote(l, 0, s1.at[l, to], r1.at[l, z], (2 * to + c, cb)).start()
        r1[l, z] = s1[l, z]
        if l == 0:
            prepare_rest()
        wait_bytes(ph_recv.at[l, 0], r1.at[l, pl.ds(0, NZ - 1)])
        total = jnp.sum(r1[l].astype(F32), axis=0)
        square_sum = total[UZ : UZ + 1, :] + total[UZ + 1 : UZ + 2, :]
        inverse_rms = lax.rsqrt(square_sum / width + EPS)
        gate = total[:UP] * inverse_rms * prm[l]
        up = total[UP:] * inverse_rms * prm[2 + l]
        taps = [prm[6 + 3 * l + j] for j in range(3)]
        conv = prm[4 + l] + taps[0] * shifted(gate, 2) + taps[1] * shifted(gate, 1) + taps[2] * gate
        hidden = (conv / (1.0 + jnp.exp(-conv))) * up
        r2[l, z] = hidden.astype(BF16)
        for d in ring:
            remote(l, 1, r2.at[l, z], r2.at[l, z], zpeer(d)).start()
        ex[3 if l == 0 else 7].wait_recv()
        if l == 0:
            ex[4].wait_recv()
        wait_bytes(ph_recv.at[l, 1], r2.at[l, pl.ds(0, NZ - 1)])
        act = r2[l].astype(F32).reshape(NZ * UP, T).astype(BF16)
        s3[l] = nn(w2[l], act).reshape(NB, FB, T).astype(BF16)
        for off in plane:
            to = plane_index(off)
            remote(l, 2, s3.at[l, to], r3.at[l, cb], (ra, to)).start()
        r3[l, cb] = s3[l, cb]
        wait_bytes(ph_recv.at[l, 2], r3.at[l, pl.ds(0, NB - 1)])
        branch = jnp.sum(r3[l].astype(F32), axis=0)
        branch = branch * dsT[l, pl.ds(pl.multiple_of(cb * FB, FB), FB), :]
        fresh = (KEEP * hT[l, cb].astype(F32) + branch).astype(BF16)
        if l == 0:
            hT[1, cb] = fresh
            for off in plane:
                remote(l, 3, hT.at[1, cb], hT.at[1, cb], (ra, plane_index(off))).start()
            wait_bytes(ph_recv.at[l, 3], hT.at[1, pl.ds(0, NB - 1)])
        else:
            half = lax.div(cb, HB)
            slot = lax.rem(cb, HB)
            owner = 2 * z + half
            hn_send[...] = fresh
            for off in plane:
                remote(l, 3, hn_send, fin.at[c, slot], (owner, plane_index(off))).start()

            @pl.when(half == c)
            def _():
                fin[c, slot] = fresh
                wait_bytes(ph_recv.at[1, 3], r3.at[0, pl.ds(0, NB - 1)])

            @pl.when(half != c)
            def _():
                remote(l, 3, hn_send, fin.at[c, slot], (owner, cb)).start()
                wait_bytes(ph_recv.at[1, 3], r3.at[0])

    out_ref[...] = fin[...]

    for copy in ex:
        copy.wait_send()
    for l in range(2):
        wait_bytes(ph_send.at[l, 0], s1.at[l, pl.ds(0, NZ - 1)])
        wait_bytes(ph_send.at[l, 1], r2.at[l, pl.ds(0, NZ - 1)])
        wait_bytes(ph_send.at[l, 2], s3.at[l, pl.ds(0, NB - 1)])
    wait_bytes(ph_send.at[0, 3], r3.at[0, pl.ds(0, NB - 1)])

    @pl.when(lax.div(cb, HB) == c)
    def _():
        wait_bytes(ph_send.at[1, 3], r3.at[0, pl.ds(0, NB - 1)])

    @pl.when(lax.div(cb, HB) != c)
    def _():
        wait_bytes(ph_send.at[1, 3], r3.at[0])


def solution(mesh, planes=(8, 4)):
    NY, NX = planes
    NZ = mesh.shape["ra"] // 2
    NB = NY * NX

    def step(*args):
        tokens, norm_gain, gate_weight = args[:3]
        _, T, FC = tokens.shape
        U = gate_weight.shape[2]
        UP = -(-(U // NZ + 2) // 8) * 8
        width = FC * mesh.shape["ra"]
        FB = 2 * FC // NB
        HB = NB // 2
        cfg = (NZ, NY, NX, FC, U, UP, T, width)
        out = pl.pallas_call(
            functools.partial(kernel, cfg),
            out_shape=jax.ShapeDtypeStruct((2, HB, FB, T), BF16),
            in_specs=[pl.BlockSpec(memory_space=pl.ANY)] * len(args),
            out_specs=pl.BlockSpec(memory_space=pltpu.VMEM),
            scratch_shapes=[pltpu.VMEM(a.shape, a.dtype) for a in args]
            + [
                pltpu.VMEM((HB, FB, T), BF16),
                pltpu.VMEM((2, NB, FB, T), BF16),
                pltpu.VMEM((2, 2 * FC, T), F32),
                pltpu.VMEM((2, 2 * FC, T), F32),
                pltpu.VMEM((2, 2, NZ * 2 * UP, FC), BF16),
                pltpu.VMEM((2, 2 * FC, NZ * UP), BF16),
                pltpu.VMEM((12, UP, T), F32),
                pltpu.VMEM((2, NZ, 2 * UP, T), BF16),
                pltpu.VMEM((2, NZ, 2 * UP, T), BF16),
                pltpu.VMEM((2, NZ, UP, T), BF16),
                pltpu.VMEM((2, NB, FB, T), BF16),
                pltpu.VMEM((2, NB, FB, T), BF16),
                pltpu.VMEM((FB, T), BF16),
                pltpu.VMEM((2, HB, FB, T), BF16),
                pltpu.SemaphoreType.DMA((len(args),)),
                pltpu.SemaphoreType.DMA((8,)),
                pltpu.SemaphoreType.DMA((8,)),
                pltpu.SemaphoreType.DMA((2, 4)),
                pltpu.SemaphoreType.DMA((2, 4)),
            ],
            compiler_params=pltpu.CompilerParams(collective_id=0, has_side_effects=True),
        )(*args)
        return jnp.transpose(out.reshape(2, FC, T), (0, 2, 1))

    in_specs = (
        P(None, None, "ra"),
        P(None, "ra"),
        P(None, "ra", "cb"),
        P(None, "cb"),
        P(None, "ra", "cb"),
        P(None, "cb"),
        P(None, None, "cb"),
        P(None, "cb"),
        P(None, "cb", "ra"),
        P(None, "ra"),
    )
    return jax.shard_map(
        step, mesh=mesh, in_specs=in_specs, out_specs=P(None, None, "ra"), check_vma=False
    )
```

time: 360 us -> 79.6 us (0.22)
  the two profiles are of different devices: /device:TPU:24 before, /device:TPU:1 now
where the time goes in v1:
time: 79.6 us; the launch traced here: 79.4 us
  Pallas kernels  73.7 us (93%)
  local copies, waits for them, and re-layouts  5.69 us (7%)
    pallas_call x1, Pallas kernels, step(): pl.pallas_call(functools.partial(kernel, cfg), out_shape=jax.ShapeDtypeSt...  73.7 us
    unnamed x5, local copies, waits for them, and re-layouts  4.12 us

profile of v1, /device:TPU:1, one launch (start us, length us, event | category | flops | bytes accessed | tf_op | source)
XLA Modules:
  0.0 79.4 jit_solution(5596412909625031041)
XLA Ops:
  0.0 1.3 %copy.13.cw_h = f32[2,3,264]{2,1,0:T(4,128)} copy(f32[2,3,264]{2,0,1:T(2,128)} %param.16) | data formatting | bytes 12672 | tf_op args[6]
  1.3 0.0 copy-start
  1.3 1.9 %copy.11.wg_h = f32[2,128,264]{2,1,0:T(8,128)} copy(f32[2,128,264]{1,2,0:T(8,128)} %param.12) | data formatting | bytes 540672 | tf_op args[2]
  3.2 0.0 copy-done
  3.2 0.9 %copy.12.wu_h = f32[2,128,264]{2,1,0:T(8,128)} copy(f32[2,128,264]{1,2,0:T(8,128)S(1)} %copy-done) | data formatting | bytes 540672 | tf_op args[4]
  4.1 73.7 %shard_map.100 = bf16[2,16,8,128]{3,2,1,0:T(8,128)(2,1)} custom-call(bf16[2,128,128]{2,1,0:T(8,128)(2,1)} %tok_h.1, f32[2,128]{1,0:T(2,128)} %g_h.1, f32[2,128,264]{2,1,0:T(8,128)} %copy.11.wg_h, f32[2,264]{1,0:T(2,128)} %gs_h.1, f32[2,128,264]{2,1,0:T(8,128)} %copy.12.wu_h, f32[2,264]{1,0:T(2,128)} %us_h.1, f32[2,3,264]{2,1,0:T(4,128)} %copy.13.cw_h, ...), custom_call_target="tpu_custom_call" | custom-call | tf_op jit(solution)/shard_map/pallas_call | solution.py:295
  77.8 1.6 %copy.14 = bf16[2,128,128]{1,2,0:T(8,128)(2,1)} copy(bf16[2,128,128]{2,1,0:T(8,128)(2,1)} %bitcast.2) | data formatting | bytes 131072 | tf_op jit(solution)/shard_map/reshape | solution.py:324
Async XLA Ops:
  1.3 1.9 %copy-start = (f32[2,128,264]{1,2,0:T(8,128)S(1)}, f32[2,128,264]{1,2,0:T(8,128)}, u32[]{:S(2)}) copy-start(f32[2,128,264]{1,2,0:T(8,128)} %param.14) | copy-start | bytes 811012
